TPU v7x, 32 devices: a whole 2x2x4 slice. The times are simulated.
32 devices in a mesh: fs: 8 (over z, y), tp: 4 (over x, core).
Axes of the slice: x: 2, y: 2, z: 4, core: 2. Of those that a mesh axis runs over, the one named last changes fastest.
Arguments:
- tokens: bfloat16 [4096, 2048], P(('fs', 'tp')), may hold values from -6 to 6
- pre_gain: float32 [2048], replicated, may hold values from 0.1 to 1.9
- w_expand: bfloat16 [2048, 8192], P('fs', 'tp'), may hold values from -0.125 to 0.125
- w_reduce: bfloat16 [8192, 2048], P('tp', 'fs'), may hold values from -0.0625 to 0.0625
- post_gain: float32 [2048], replicated, may hold values from 0.1 to 1.9
Outputs:
- result: bfloat16 [4096, 2048], P(('fs', 'tp'))
All inputs are finite; a program needn't handle non-finite values.
Results may differ from a plain program's by a relative error of at most 0.014.
Values may be sent and summed in bfloat16 or wider, within the bound.
A program may use at most 64 MiB of HBM per device.

v0:
```python
import jax
import jax.numpy as jnp
from jax import lax
from jax.sharding import PartitionSpec as P

NORM_EPS = 1e-06


def rms_scale(values, gain_row):
    widened = values.astype(jnp.float32)
    scaled = widened * lax.rsqrt(jnp.mean(widened * widened, axis=-1, keepdims=True) + NORM_EPS)
    return scaled * gain_row


def squared_relu(preact):
    return jnp.square(jnp.maximum(preact, 0.0)).astype(jnp.bfloat16)


def per_device(tokens, pre_gain, w_expand, w_reduce, post_gain):
    normed = rms_scale(tokens, pre_gain).astype(jnp.bfloat16)
    expand_full = lax.all_gather(w_expand, "fs", axis=0, tiled=True)
    hidden = squared_relu(
        jnp.dot(
            lax.all_gather(normed, "tp", axis=0, tiled=True),
            expand_full,
            preferred_element_type=jnp.float32,
        )
    )
    reduce_full = lax.all_gather(w_reduce, "fs", axis=1, tiled=True)
    mixed = lax.psum_scatter(
        jnp.dot(hidden, reduce_full, preferred_element_type=jnp.float32).astype(jnp.bfloat16),
        "tp",
        scatter_dimension=0,
        tiled=True,
    )
    return rms_scale(mixed, post_gain).astype(jnp.bfloat16)


def solution(mesh):
    return jax.shard_map(
        per_device,
        mesh=mesh,
        in_specs=(P(("fs", "tp"), None), P(), P("fs", "tp"), P("tp", "fs"), P()),
        out_specs=P(("fs", "tp"), None),
        check_vma=False,
    )
```

profile of v0, /device:TPU:0, one launch (start us, length us, event | category | flops | bytes accessed | tf_op | source)
XLA Modules:
  0.0 342.9 jit_solution(1764702396853761959)
XLA Ops:
  6.5 0.0 all-gather.4.cloned.1.call-start
  6.5 1.2 fusion
  7.8 2.0 fusion.2
  9.8 0.0 all-gather.4.cloned.1.call-update
  9.8 0.0 all-gather.6.cloned.1.call-start
  9.9 0.7 all-gather.6.cloned.1.call-update
  10.6 0.0 all-gather.8.cloned.1.call-start
  10.6 0.7 all-gather.8.cloned.1.call-update
  11.3 0.0 copy-start
  11.3 0.0 reduce-scatter.2.cloned.1.call-start
  11.4 23.9 %all-gather.4.cloned.1.call-done = bf16[512,2048]{1,0:T(8,128)(2,1)} async-done(((bf16[128,2048]{1,0:T(8,128)(2,1)}), bf16[512,2048]{1,0:T(8,128)(2,1)}) %all-gather.4.cloned.1.call-update) | async-done | bytes 2097168 | tf_op jit(solution)/shard_map/all_gather | solution.py:24
  35.3 126.6 %all-gather.6.cloned.1.call-done = bf16[2048,2048]{1,0:T(8,128)(2,1)} async-done(((bf16[256,2048]{1,0:T(8,128)(2,1)}), bf16[2048,2048]{1,0:T(8,128)(2,1)}) %all-gather.6.cloned.1.call-update) | async-done | bytes 8388624 | tf_op jit(solution)/shard_map/all_gather | solution.py:21
  161.9 125.2 %all-gather.8.cloned.1.call-done = bf16[2048,2048]{1,0:T(8,128)(2,1)} async-done(((bf16[2048,256]{1,0:T(8,128)(2,1)}), bf16[2048,2048]{1,0:T(8,128)(2,1)}) %all-gather.8.cloned.1.call-update) | async-done | bytes 8388624 | tf_op jit(solution)/shard_map/all_gather | solution.py:29
  287.1 16.5 %convolution_convert_fusion = bf16[512,2048]{1,0:T(8,128)(2,1)} fusion(bf16[2048,2048]{1,0:T(8,128)(2,1)} %all-gather.8.cloned.1.call-done, bf16[512,2048]{1,0:T(8,128)(2,1)} %all-gather.4.cloned.1.call-done, bf16[2048,2048]{1,0:T(8,128)(2,1)} %all-gather.6.cloned.1.call-done), kind=kOutput, calls=%fused_computation.1 | convolution fusion | flops 8594128896 | bytes 20971520 | tf_op jit(solution)/shard_map/dot_general | solution.py:31
  303.6 0.0 reduce-scatter.2.cloned.1.call-update
  303.6 29.5 %reduce-scatter.2.cloned.1.call-done = bf16[128,2048]{1,0:T(8,128)(2,1)} async-done(((bf16[512,2048]{1,0:T(8,128)(2,1)}), bf16[128,2048]{1,0:T(8,128)(2,1)}) %reduce-scatter.2.cloned.1.call-update) | async-done | bytes 524304 | tf_op jit(solution)/shard_map/reduce_scatter | solution.py:30
  333.1 1.2 fusion.3
  334.4 0.0 copy-done
  334.4 2.0 fusion.5
  (2 shorter events, 0.0 us)
Async XLA Ops:
  6.5 28.7 %all-gather.4.cloned.1.call-start = ((), (), s32[]{:S(2)}) async-start(), calls=%async_computation.1 | async-start | bytes 2621440 | tf_op jit(solution)/shard_map/all_gather | solution.py:24
  9.8 152.1 %all-gather.6.cloned.1.call-start = ((), (), s32[]{:S(2)}) async-start(), calls=%async_computation.2 | async-start | bytes 9437184 | tf_op jit(solution)/shard_map/all_gather | solution.py:21
  10.6 276.5 %all-gather.8.cloned.1.call-start = ((), (), s32[]{:S(2)}) async-start(), calls=%async_computation.3 | async-start | bytes 9437184 | tf_op jit(solution)/shard_map/all_gather | solution.py:29
  11.3 323.0 %copy-start = (f32[2048]{0:T(1024)S(1)}, f32[2048]{0:T(1024)}, u32[]{:S(2)}) copy-start(f32[2048]{0:T(1024)} %param.9) | copy-start | bytes 24580
  11.3 321.8 %reduce-scatter.2.cloned.1.call-start = ((), (), s32[]{:S(2)}) async-start(), calls=%async_computation.4 | async-start | bytes 2621440 | tf_op jit(solution)/shard_map/reduce_scatter | solution.py:30
Sparse Core Ops, SparseCore 0:
  9.9 25.2 all-gather.3
  37.4 124.4 all-gather.5
  164.0 123.1 all-gather.7
  303.8 29.3 reduce-scatter.1
where the time goes:
time: 343 us
  waiting for transfers between devices  307 us (90%)
  matrix products  16.5 us (5%)
  between operations  13.1 us (4%)
  other arithmetic  6.53 us (2%)
    all_gather x1, waiting for transfers between devices, per_device(): expand_full = lax.all_gather(w_expand, 'fs', axis=0, tiled=True)  127 us
    all_gather x1, waiting for transfers between devices, per_device(): reduce_full = lax.all_gather(w_reduce, 'fs', axis=1, tiled=True)  125 us
    reduce_scatter x1, waiting for transfers between devices, per_device(): lax.psum_scatter(jnp.dot(hidden, reduce_full, preferred_element_type=jnp....  29.5 us
    all_gather x1, waiting for transfers between devices, per_device(): lax.all_gather(normed, 'tp', axis=0, tiled=True)  23.9 us
    dot_general x1, matrix products, per_device(): jnp.dot(hidden, reduce_full, preferred_element_type=jnp.float32)  16.5 us
  transfers between devices with their start and end apart: 4, of which 4 were waited for; matrix products, arithmetic and copies ran while one was open for 0% of the time, Pallas kernels for 0%

commit v1 on v0

--- a/solution.py
+++ b/solution.py
@@ -18,7 +18,14 @@
 
 def per_device(tokens, pre_gain, w_expand, w_reduce, post_gain):
     normed = rms_scale(tokens, pre_gain).astype(jnp.bfloat16)
-    expand_full = lax.all_gather(w_expand, "fs", axis=0, tiled=True)
+    count = lax.axis_size("fs")
+    right = [(i, (i + 1) % count) for i in range(count)]
+    shards = [w_expand]
+    for stride in range(1, count):
+        shards = [lax.ppermute(shards[0], "fs", right), *shards]
+    full = jnp.concatenate(shards, axis=0)
+    shift = (lax.axis_index("fs") + 1) * shards[-1].shape[0]
+    expand_full = jnp.roll(full, shift, axis=0)
     hidden = squared_relu(
         jnp.dot(
             lax.all_gather(normed, "tp", axis=0, tiled=True),

time: 343 us -> 372 us (1.085)
  local copies, waits for them, and re-layouts: 0.01 us -> 29 us
  waiting for transfers between devices: 307 us -> 303 us
    ppermute x0 -> x7, waiting for transfers between devices: none -> 270 us  [per_device(): shards = [lax.ppermute(shards[0], 'fs', right), *shards]]
    all_gather x1 -> x0, waiting for transfers between devices: 127 us -> none  [per_device(): expand_full = lax.all_gather(w_expand, 'fs', axis=0, tiled=True)]
    all_gather x1, waiting for transfers between devices: 125 us -> 0.01 us  [per_device(): reduce_full = lax.all_gather(w_reduce, 'fs', axis=1, tiled=True)]
    unnamed x2 -> x31, local copies, waits for them, and re-layouts: 0.01 us -> 27.9 us
    all_gather x1, waiting for transfers between devices: 23.9 us -> 0.01 us  [per_device(): lax.all_gather(normed, 'tp', axis=0, tiled=True)]
  transfers between devices with their start and end apart: 4 -> 10, of which waited for: 4 -> 8; matrix products, arithmetic and copies ran while one was open for 0% -> 7% of each run, Pallas kernels for 0% -> 0%
where the time goes in v1:
time: 372 us; the launch traced here: 371 us
  waiting for transfers between devices  303 us (81%)
  local copies, waits for them, and re-layouts  29 us (8%)
  matrix products  16.5 us (4%)
  between operations  13.1 us (4%)
  other arithmetic  6.61 us (2%)
    ppermute x7, waiting for transfers between devices, per_device(): shards = [lax.ppermute(shards[0], 'fs', right), *shards]  270 us
    reduce_scatter x1, waiting for transfers between devices, per_device(): lax.psum_scatter(jnp.dot(hidden, reduce_full, preferred_element_type=jnp....  31.8 us
    unnamed x31, local copies, waits for them, and re-layouts  27.9 us
    dot_general x1, matrix products, per_device(): jnp.dot(hidden, reduce_full, preferred_element_type=jnp.float32)  16.5 us
  transfers between devices with their start and end apart: 10, of which 8 were waited for; matrix products, arithmetic and copies ran while one was open for 7% of the time, Pallas kernels for 0%

profile of v1, /device:TPU:0, one launch (start us, length us, event | category | flops | bytes accessed | tf_op | source)
XLA Modules:
  0.0 371.3 jit_solution(9016899625961913129)
XLA Ops:
  6.5 1.3 fusion.4
  7.9 2.0 fusion.6
  10.7 3.0 collective-permute-start
  13.8 26.4 %collective-permute-done = bf16[256,2048]{1,0:T(8,128)(2,1)S(1)} collective-permute-done((bf16[256,2048]{1,0:T(8,128)(2,1)}, bf16[256,2048]{1,0:T(8,128)(2,1)S(1)}, u32[]{:S(2)}, u32[]{:S(2)}) %collective-permute-start) | collective-permute-done | bytes 1048608 | tf_op jit(solution)/shard_map/ppermute | solution.py:25
  40.2 42.9 %collective-permute-done.1 = bf16[256,2048]{1,0:T(8,128)(2,1)S(1)} collective-permute-done((bf16[256,2048]{1,0:T(8,128)(2,1)S(1)}, bf16[256,2048]{1,0:T(8,128)(2,1)S(1)}, u32[]{:S(2)}, u32[]{:S(2)}) %collective-permute-start.1) | collective-permute-done | bytes 1048608 | tf_op jit(solution)/shard_map/ppermute | solution.py:25
  83.1 40.4 %collective-permute-done.2 = bf16[256,2048]{1,0:T(8,128)(2,1)S(1)} collective-permute-done((bf16[256,2048]{1,0:T(8,128)(2,1)S(1)}, bf16[256,2048]{1,0:T(8,128)(2,1)S(1)}, u32[]{:S(2)}, u32[]{:S(2)}) %collective-permute-start.2) | collective-permute-done | bytes 1048608 | tf_op jit(solution)/shard_map/ppermute | solution.py:25
  124.4 50.3 %collective-permute-done.3 = bf16[256,2048]{1,0:T(8,128)(2,1)S(1)} collective-permute-done((bf16[256,2048]{1,0:T(8,128)(2,1)S(1)}, bf16[256,2048]{1,0:T(8,128)(2,1)S(1)}, u32[]{:S(2)}, u32[]{:S(2)}) %collective-permute-start.3) | collective-permute-done | bytes 1048608 | tf_op jit(solution)/shard_map/ppermute | solution.py:25
  174.8 1.0 copy-done.3
  175.8 50.1 %collective-permute-done.4 = bf16[256,2048]{1,0:T(8,128)(2,1)S(1)} collective-permute-done((bf16[256,2048]{1,0:T(8,128)(2,1)S(1)}, bf16[256,2048]{1,0:T(8,128)(2,1)S(1)}, u32[]{:S(2)}, u32[]{:S(2)}) %collective-permute-start.4) | collective-permute-done | bytes 1048608 | tf_op jit(solution)/shard_map/ppermute | solution.py:25
  225.8 1.0 copy-done.5
  226.9 32.6 %collective-permute-done.5 = bf16[256,2048]{1,0:T(8,128)(2,1)} collective-permute-done((bf16[256,2048]{1,0:T(8,128)(2,1)S(1)}, bf16[256,2048]{1,0:T(8,128)(2,1)}, u32[]{:S(2)}, u32[]{:S(2)}) %collective-permute-start.5) | collective-permute-done | bytes 1048608 | tf_op jit(solution)/shard_map/ppermute | solution.py:25
  259.4 27.8 %collective-permute-done.6 = bf16[256,2048]{1,0:T(8,128)(2,1)} collective-permute-done((bf16[256,2048]{1,0:T(8,128)(2,1)}, bf16[256,2048]{1,0:T(8,128)(2,1)}, u32[]{:S(2)}, u32[]{:S(2)}) %collective-permute-start.6) | collective-permute-done | bytes 1048608 | tf_op jit(solution)/shard_map/ppermute | solution.py:25
  287.2 2.3 constant_dynamic-update-slice_fusion.15
  289.5 2.3 constant_dynamic-update-slice_fusion.14
  291.8 2.3 constant_dynamic-update-slice_fusion.13
  294.2 2.3 constant_dynamic-update-slice_fusion.12
  296.5 2.3 constant_dynamic-update-slice_fusion.11
  298.8 1.1 constant_dynamic-update-slice_fusion.10
  299.9 1.1 constant_dynamic-update-slice_fusion.9
  300.9 1.1 constant_dynamic-update-slice_fusion.8
  302.1 2.4 constant_dynamic-update-slice_fusion.7
  304.5 2.3 constant_dynamic-update-slice_fusion.6
  306.8 1.0 constant_dynamic-update-slice_fusion.5
  307.8 1.1 constant_dynamic-update-slice_fusion.4
  308.9 1.1 constant_dynamic-update-slice_fusion.3
  310.0 1.0 constant_dynamic-update-slice_fusion.2
  311.0 1.1 constant_dynamic-update-slice_fusion.1
  312.1 1.1 constant_dynamic-update-slice_fusion
  313.2 16.5 %convolution_convert_fusion = bf16[512,2048]{1,0:T(8,128)(2,1)} fusion(bf16[2048,2048]{1,0:T(8,128)(2,1)} %all-gather.5.cloned.1.call-done, bf16[512,2048]{1,0:T(8,128)(2,1)} %all-gather.3.cloned.1.call-done, bf16[4096,2048]{1,0:T(8,128)(2,1)} %constant_dynamic-update-slice_fusion, s32[]{:T(128)S(6)} %select_n.14), kind=kOutput, calls=%fused_computation.3 | convolution fusion | flops 8594128896 | bytes 20971524 | tf_op jit(solution)/shard_map/dot_general | solution.py:38
  329.7 31.8 %reduce-scatter.2.cloned.1.call-done = bf16[128,2048]{1,0:T(8,128)(2,1)} async-done(((bf16[512,2048]{1,0:T(8,128)(2,1)}), bf16[128,2048]{1,0:T(8,128)(2,1)}) %reduce-scatter.2.cloned.1.call-update) | async-done | bytes 524304 | tf_op jit(solution)/shard_map/reduce_scatter | solution.py:37
  361.5 1.2 fusion.7
  362.7 2.0 fusion.9
  (30 shorter events, 1.8 us)
Async XLA Ops:
  6.5 294.4 %copy-start = (bf16[256,2048]{1,0:T(8,128)(2,1)S(1)}, bf16[256,2048]{1,0:T(8,128)(2,1)}, u32[]{:S(2)}) copy-start(bf16[256,2048]{1,0:T(8,128)(2,1)} %param.7) | copy-start | bytes 3145732
  6.5 306.6 %all-gather.3.cloned.1.call-start = ((), (), s32[]{:S(2)}) async-start(), calls=%async_computation.1 | async-start | bytes 2621440 | tf_op jit(solution)/shard_map/all_gather | solution.py:31
  9.9 303.3 %all-gather.5.cloned.1.call-start = ((), (), s32[]{:S(2)}) async-start(), calls=%async_computation.2 | async-start | bytes 9437184 | tf_op jit(solution)/shard_map/all_gather | solution.py:36
  10.7 350.8 %reduce-scatter.2.cloned.1.call-start = ((), (), s32[]{:S(2)}) async-start(), calls=%async_computation.3 | async-start | bytes 2621440 | tf_op jit(solution)/shard_map/reduce_scatter | solution.py:37
  10.7 29.5 %collective-permute-start = (bf16[256,2048]{1,0:T(8,128)(2,1)}, bf16[256,2048]{1,0:T(8,128)(2,1)S(1)}, u32[]{:S(2)}, u32[]{:S(2)}) collective-permute-start(bf16[256,2048]{1,0:T(8,128)(2,1)} %param.7), channel_id=1, source_target_pairs={{0,4},{4,8},{8,12},{12,16},{16,20},{20,24},{24,28},{28,0},{1,5},{5... | collective-permute-start | bytes 3145736 | tf_op jit(solution)/shard_map/ppermute | solution.py:25
  40.2 42.9 %collective-permute-start.1 = (bf16[256,2048]{1,0:T(8,128)(2,1)S(1)}, bf16[256,2048]{1,0:T(8,128)(2,1)S(1)}, u32[]{:S(2)}, u32[]{:S(2)}) collective-permute-start(bf16[256,2048]{1,0:T(8,128)(2,1)S(1)} %collective-permute-done), channel_id=1, source_target_pairs={{0,4},{4,8},{8,12},{12,16},{16,20},{20,24},{24,28},{28,0},{1,5},{5... | collective-permute-start | bytes 3145736 | tf_op jit(solution)/shard_map/ppermute | solution.py:25
  83.1 40.4 %collective-permute-start.2 = (bf16[256,2048]{1,0:T(8,128)(2,1)S(1)}, bf16[256,2048]{1,0:T(8,128)(2,1)S(1)}, u32[]{:S(2)}, u32[]{:S(2)}) collective-permute-start(bf16[256,2048]{1,0:T(8,128)(2,1)S(1)} %collective-permute-done.1), channel_id=1, source_target_pairs={{0,4},{4,8},{8,12},{12,16},{16,20},{20,24},{24,28},{28,0},{1,5},{5... | collective-permute-start | bytes 3145736 | tf_op jit(solution)/shard_map/ppermute | solution.py:25
  123.5 1.0 copy-start.1
  124.4 50.3 %collective-permute-start.3 = (bf16[256,2048]{1,0:T(8,128)(2,1)S(1)}, bf16[256,2048]{1,0:T(8,128)(2,1)S(1)}, u32[]{:S(2)}, u32[]{:S(2)}) collective-permute-start(bf16[256,2048]{1,0:T(8,128)(2,1)S(1)} %collective-permute-done.2), channel_id=1, source_target_pairs={{0,4},{4,8},{8,12},{12,16},{16,20},{20,24},{24,28},{28,0},{1,5},{5... | collective-permute-start | bytes 3145736 | tf_op jit(solution)/shard_map/ppermute | solution.py:25
  174.7 1.0 copy-start.3
  175.7 50.1 %collective-permute-start.4 = (bf16[256,2048]{1,0:T(8,128)(2,1)S(1)}, bf16[256,2048]{1,0:T(8,128)(2,1)S(1)}, u32[]{:S(2)}, u32[]{:S(2)}) collective-permute-start(bf16[256,2048]{1,0:T(8,128)(2,1)S(1)} %collective-permute-done.3), channel_id=1, source_target_pairs={{0,4},{4,8},{8,12},{12,16},{16,20},{20,24},{24,28},{28,0},{1,5},{5... | collective-permute-start | bytes 3145736 | tf_op jit(solution)/shard_map/ppermute | solution.py:25
  225.8 1.1 copy-start.5
  226.9 32.6 %collective-permute-start.5 = (bf16[256,2048]{1,0:T(8,128)(2,1)S(1)}, bf16[256,2048]{1,0:T(8,128)(2,1)}, u32[]{:S(2)}, u32[]{:S(2)}) collective-permute-start(bf16[256,2048]{1,0:T(8,128)(2,1)S(1)} %collective-permute-done.4), channel_id=1, source_target_pairs={{0,4},{4,8},{8,12},{12,16},{16,20},{20,24},{24,28},{28,0},{1,5},{5... | collective-permute-start | bytes 3145736 | tf_op jit(solution)/shard_map/ppermute | solution.py:25
  259.4 27.8 %collective-permute-start.6 = (bf16[256,2048]{1,0:T(8,128)(2,1)}, bf16[256,2048]{1,0:T(8,128)(2,1)}, u32[]{:S(2)}, u32[]{:S(2)}) collective-permute-start(bf16[256,2048]{1,0:T(8,128)(2,1)} %collective-permute-done.5), channel_id=1, source_target_pairs={{0,4},{4,8},{8,12},{12,16},{16,20},{20,24},{24,28},{28,0},{1,5},{5... | collective-permute-start | bytes 3145736 | tf_op jit(solution)/shard_map/ppermute | solution.py:25
  259.4 47.3 %copy-start.6 = (bf16[256,2048]{1,0:T(8,128)(2,1)S(1)}, bf16[256,2048]{1,0:T(8,128)(2,1)}, u32[]{:S(2)}) copy-start(bf16[256,2048]{1,0:T(8,128)(2,1)} %copy-done.5) | copy-start | bytes 3145732
  259.4 48.4 %copy-start.4 = (bf16[256,2048]{1,0:T(8,128)(2,1)S(1)}, bf16[256,2048]{1,0:T(8,128)(2,1)}, u32[]{:S(2)}) copy-start(bf16[256,2048]{1,0:T(8,128)(2,1)} %copy-done.3) | copy-start | bytes 3145732
  259.4 49.4 %copy-start.2 = (bf16[256,2048]{1,0:T(8,128)(2,1)S(1)}, bf16[256,2048]{1,0:T(8,128)(2,1)}, u32[]{:S(2)}) copy-start(bf16[256,2048]{1,0:T(8,128)(2,1)} %copy-done.1) | copy-start | bytes 3145732
  313.2 49.6 %copy-start.7 = (f32[2048]{0:T(1024)S(1)}, f32[2048]{0:T(1024)}, u32[]{:S(2)}) copy-start(f32[2048]{0:T(1024)} %param.9) | copy-start | bytes 24580
Sparse Core Ops, SparseCore 0:
  10.0 25.2 all-gather.2
  37.4 192.9 all-gather.4
  329.8 31.6 reduce-scatter.1
